TPU v7x, 512 devices: a whole 4x4x16 slice. The times are simulated.
512 devices in a mesh: sp: 16 (over y, x), tp: 32 (over z, core).
Axes of the slice: x: 4, y: 4, z: 16, core: 2. Of those that a mesh axis runs over, the one named last changes fastest.
Arguments:
- tokens: bfloat16 [3, 8192, 4096], P(None, 'sp', 'tp'), may hold values from -6 to 6
- new_token: bfloat16 [3, 1, 4096], P(None, None, 'tp'), may hold values from -6 to 6
- query_weight: bfloat16 [4096, 4096], P(None, 'tp'), may hold values from -0.09375 to 0.09375
- key_weight: bfloat16 [4096, 4096], P(None, 'tp'), may hold values from -0.09375 to 0.09375
- value_weight: bfloat16 [4096, 4096], P(None, 'tp'), may hold values from -0.09375 to 0.09375
- log_decay: float32 [64], P('tp'), may hold values from -0.034 to 0
Outputs:
- state: bfloat16 [3, 64, 64, 64], P(None, 'tp', 'sp')
- read: bfloat16 [3, 4096], P(None, 'tp')
All inputs are finite; a program needn't handle non-finite values.
Results may differ from a plain program's by a relative error of at most 0.012.
Values may be sent and summed in bfloat16 or wider, within the bound.
No kernel may reach another device: no remote copies, remote signals or barrier semaphores. Data moves between devices by JAX's collectives and lax.ppermute only.
A program may use at most 64 MiB of HBM per device.

v0:
```python
import jax
import jax.numpy as jnp
from jax import lax
from jax.sharding import PartitionSpec as P

HD = 64


def cut_along(value, dim, count):
    dims = value.shape
    tiles = value.reshape(*dims[:dim], count, dims[dim] // count, *dims[dim + 1 :])
    return jnp.moveaxis(tiles, dim, 0)


def sent_and_summed(value, axis, dim):
    tiles = cut_along(value, dim, lax.axis_size(axis))
    arrived = lax.all_to_all(tiles, axis, split_axis=0, concat_axis=0, tiled=True)
    return arrived.sum(axis=0)


def from_everyone(value, axis):
    copies = jnp.broadcast_to(value, (lax.axis_size(axis), *value.shape))
    return lax.all_to_all(copies, axis, split_axis=0, concat_axis=0, tiled=True)


def over_copies(value, axis):
    everything = from_everyone(value, axis)
    return jnp.sum(everything, axis=0)


def rotate(values, positions):
    half_dim = values.shape[-1] // 2
    inverse = 10000.0 ** (-jnp.arange(half_dim, dtype=jnp.float32) / half_dim)
    angles = positions.astype(jnp.float32)[:, None, None] * inverse[None, None, :]
    cosine = jnp.cos(angles)
    sine_part = jnp.sin(angles)
    first = values[..., :half_dim]
    second = values[..., half_dim:]
    return jnp.concatenate(
        [first * cosine - second * sine_part, first * sine_part + second * cosine], axis=-1
    )


def group_norm(output):
    centered = output - jnp.mean(output, axis=-1, keepdims=True)
    return centered * lax.rsqrt(jnp.mean(centered * centered, axis=-1, keepdims=True) + 1e-05)


def body(tokens, new_token, query_weight, key_weight, value_weight, log_decay):
    sequences, span_len, _ = tokens.shape
    head_count = log_decay.shape[0]
    inner = head_count * HD
    groups = lax.axis_size("sp")
    own_index = lax.axis_index("sp")
    key_scale = HD ** (-0.5)
    row_weights = jnp.concatenate([key_weight, value_weight], axis=1)
    all_weights = jnp.concatenate([key_weight, value_weight, query_weight], axis=1)
    row_piece = lax.all_gather(tokens, "tp", axis=2, tiled=True)
    new_piece = lax.all_gather(new_token, "tp", axis=2, tiled=True)
    row_total = jnp.dot(row_piece, row_weights, preferred_element_type=jnp.float32)
    new_total = jnp.dot(new_piece, all_weights, preferred_element_type=jnp.float32)
    row_total = row_total.reshape(sequences, span_len, 2, head_count, HD)
    offsets = own_index * span_len + jnp.arange(span_len, dtype=jnp.int32)
    key_rows = (rotate(row_total[:, :, 0], offsets) * key_scale).astype(jnp.bfloat16)
    value_rows = row_total[:, :, 1].astype(jnp.bfloat16)
    to_end = (span_len - 1 - jnp.arange(span_len, dtype=jnp.int32)).astype(jnp.float32)
    decay_rows = jnp.exp(to_end[:, None] * log_decay[None, :])
    weighted = (key_rows.astype(jnp.float32) * decay_rows[None, :, :, None]).astype(jnp.bfloat16)
    span_state = jnp.einsum(
        "sthk,sthv->shkv", weighted, value_rows, preferred_element_type=jnp.float32
    )
    carried_state = jnp.exp(log_decay * (span_len * (groups - 1 - own_index)).astype(jnp.float32))
    scaled_state = span_state * carried_state[None, :, None, None]
    state_rows = sent_and_summed(scaled_state, "sp", 2)
    new_total = new_total.reshape(sequences, 1, 3, head_count, HD)
    new_position = jnp.full((1,), groups * span_len, jnp.int32)
    fresh_key = (rotate(new_total[:, :, 0], new_position) * key_scale).astype(jnp.bfloat16)[:, 0]
    new_value = new_total[:, 0, 1].astype(jnp.bfloat16)
    new_query = rotate(new_total[:, :, 2], new_position).astype(jnp.bfloat16)[:, 0]
    query_entries = new_query.astype(jnp.float32)
    decay_one = jnp.exp(log_decay)[None, :, None]
    partial_read = (
        jnp.einsum("shkv,shk->shv", scaled_state, query_entries, precision=lax.Precision.HIGHEST)
        * decay_one
    )
    summed = over_copies(partial_read, "sp")
    own_term = jnp.sum(
        query_entries * fresh_key.astype(jnp.float32), axis=-1, keepdims=True
    ) * new_value.astype(jnp.float32)
    normed = group_norm(summed + own_term)
    return (state_rows.astype(jnp.bfloat16), normed.reshape(sequences, inner).astype(jnp.bfloat16))


def solution(mesh):
    return jax.shard_map(
        body,
        mesh=mesh,
        in_specs=(
            P(None, "sp", "tp"),
            P(None, None, "tp"),
            P(None, "tp"),
            P(None, "tp"),
            P(None, "tp"),
            P("tp"),
        ),
        out_specs=(P(None, "tp", "sp", None), P(None, "tp")),
        check_vma=False,
    )
```

profile of v0, /device:TPU:32, one launch (start us, length us, event | category | flops | bytes accessed | tf_op | source)
XLA Modules:
  0.0 172.4 jit_solution(1786247637780565341)
XLA Ops:
  7.2 0.7 all-gather.2.cloned.1.call-update
  7.9 1.5 copy.27
  9.4 1.4 copy.26
  10.8 34.3 %all_gather.7 = bf16[3,1,4096]{2,0,1:T(4,128)(2,1)S(1)} all-gather(bf16[3,1,128]{2,0,1:T(4,128)(2,1)S(1)} %copy-done.3), channel_id=1, replica_groups=mesh['sp'=16,'tp'=32] {'tp'}, dimensions={2}, use_global_device_ids=true | all-gather | bytes 25344 | tf_op jit(solution)/shard_map/all_gather | solution.py:59
  45.1 1.9 %fusion.9 = f32[3,384]{1,0:T(4,128)S(1)} fusion(bf16[4096,128]{1,0:T(8,128)(2,1)} %param.8, bf16[4096,128]{1,0:T(8,128)(2,1)S(1)} %copy-done, bf16[4096,128]{1,0:T(8,128)(2,1)S(1)} %copy-done.1, bf16[3,1,4096]{2,0,1:T(4,128)(2,1)S(1)} %all_gather.7), kind=kOutput, calls=%fused_computation.11 | convolution fusion | flops 18874368 | bytes 3174912 | tf_op jit(solution)/shard_map/dot_general | solution.py:61
  47.0 0.1 reshape.207
  47.4 0.3 multiply_cosine_fusion
  47.7 82.5 %all-gather.2.cloned.1.call-done = bf16[3,512,4096]{2,1,0:T(8,128)(2,1)} async-done(((bf16[3,512,128]{2,1,0:T(8,128)(2,1)}), bf16[3,512,4096]{2,1,0:T(8,128)(2,1)}) %all-gather.2.cloned.1.call-update) | async-done | bytes 12582928 | tf_op jit(solution)/shard_map/all_gather | solution.py:58
  130.3 6.8 %fusion.6 = f32[256,3,512]{2,0,1:T(8,128)S(1)} fusion(bf16[3,512,4096]{2,1,0:T(8,128)(2,1)} %all-gather.2.cloned.1.call-done, bf16[4096,128]{0,1:T(8,128)(2,1)S(1)} %copy.27, bf16[4096,128]{0,1:T(8,128)(2,1)} %copy.26), kind=kOutput, calls=%fused_computation.7 | convolution fusion | flops 3225419776 | bytes 16252928 | tf_op jit(solution)/shard_map/dot_general | solution.py:60
  137.1 0.1 multiply_subtract_fusion
  137.2 0.3 convolution_multiply_fusion
  137.5 0.2 fusion.22
  137.8 0.7 reshape.215
  138.5 6.4 %all-to-all-start.1 = ((f32[16,1,384]{2,1,0:T(1,128)}), f32[16,1,384]{2,1,0:T(1,128)S(1)}, u32[]{:S(2)}, u32[]{:S(2)}) async-start(f32[16,1,384]{2,1,0:T(1,128)} %reshape.215), calls=%async_computation.1 | async-start | bytes 49152 | tf_op jit(solution)/shard_map/all_to_all | solution.py:23
  145.0 0.2 multiply_reduce_fusion.1
  145.2 0.1 mul.280
  145.3 0.1 reshape.208
  145.4 0.8 reshape.213
  146.2 6.3 %all-to-all-done.1 = f32[16,1,384]{2,1,0:T(1,128)S(1)} async-done(((f32[16,1,384]{2,1,0:T(1,128)}), f32[16,1,384]{2,1,0:T(1,128)S(1)}, u32[]{:S(2)}, u32[]{:S(2)}) %all-to-all-start.1) | async-done | bytes 24608 | tf_op jit(solution)/shard_map/all_to_all | solution.py:23
  152.5 3.5 %all-to-all-start = ((f32[16,1,1536]{2,1,0:T(1,128)}), f32[16,1,1536]{2,1,0:T(1,128)S(1)}, u32[]{:S(2)}, u32[]{:S(2)}) async-start(f32[16,1,1536]{2,1,0:T(1,128)} %reshape.213), calls=%async_computation | async-start | bytes 196608 | tf_op jit(solution)/shard_map/all_to_all | solution.py:17
  156.1 0.5 broadcast.164
  156.6 0.7 reduce.1
  157.3 0.1 reshape.216
  157.4 0.2 fusion.32
  157.7 0.2 multiply_reduce_fusion
  157.9 0.1 mul.285
  158.1 0.1 sub.42
  158.2 0.6 multiply_convert_fusion.2
  158.7 5.1 %all-to-all-done = f32[16,1,1536]{2,1,0:T(1,128)S(1)} async-done(((f32[16,1,1536]{2,1,0:T(1,128)}), f32[16,1,1536]{2,1,0:T(1,128)S(1)}, u32[]{:S(2)}, u32[]{:S(2)}) %all-to-all-start) | async-done | bytes 98336 | tf_op jit(solution)/shard_map/all_to_all | solution.py:17
  163.8 0.9 reduce
  164.7 0.1 reshape.214
  164.9 0.7 reduce_sum.47
  (30 shorter events, 0.9 us)
Async XLA Ops:
  7.2 37.9 %copy-start = (bf16[4096,128]{1,0:T(8,128)(2,1)S(1)}, bf16[4096,128]{1,0:T(8,128)(2,1)}, u32[]{:S(2)}) copy-start(bf16[4096,128]{1,0:T(8,128)(2,1)} %param.10) | copy-start | bytes 3145732
  7.2 2.3 %copy-start.1 = (bf16[4096,128]{1,0:T(8,128)(2,1)S(1)}, bf16[4096,128]{1,0:T(8,128)(2,1)}, u32[]{:S(2)}) copy-start(bf16[4096,128]{1,0:T(8,128)(2,1)} %param.9) | copy-start | bytes 3145732
  7.2 3.6 %copy-start.3 = (bf16[3,1,128]{2,0,1:T(4,128)(2,1)S(1)}, bf16[3,1,128]{2,0,1:T(4,128)(2,1)}, u32[]{:S(2)}) copy-start(bf16[3,1,128]{2,0,1:T(4,128)(2,1)} %param.7) | copy-start | bytes 2308
  7.2 123.1 %all-gather.2.cloned.1.call-start = ((), (), s32[]{:S(2)}) async-start(), calls=%async_computation.2 | async-start | bytes 12976128 | tf_op jit(solution)/shard_map/all_gather | solution.py:58
  45.1 2.3 %copy-start.2 = (f32[2]{0:T(128)S(1)}, f32[2]{0:T(128)}, u32[]{:S(2)}) copy-start(f32[2]{0:T(128)} %param.11) | copy-start | bytes 28
  138.5 14.0 %all-to-all-start.1 = ((f32[16,1,384]{2,1,0:T(1,128)}), f32[16,1,384]{2,1,0:T(1,128)S(1)}, u32[]{:S(2)}, u32[]{:S(2)}) async-start(f32[16,1,384]{2,1,0:T(1,128)} %reshape.215), calls=%async_computation.1 | async-start | bytes 49152 | tf_op jit(solution)/shard_map/all_to_all | solution.py:23
  152.5 11.3 %all-to-all-start = ((f32[16,1,1536]{2,1,0:T(1,128)}), f32[16,1,1536]{2,1,0:T(1,128)S(1)}, u32[]{:S(2)}, u32[]{:S(2)}) async-start(f32[16,1,1536]{2,1,0:T(1,128)} %reshape.213), calls=%async_computation | async-start | bytes 196608 | tf_op jit(solution)/shard_map/all_to_all | solution.py:17
Sparse Core Ops, SparseCore 0:
  10.0 120.1 all-gather.1
where the time goes:
time: 173 us; the launch traced here: 172 us
  waiting for transfers between devices  94.6 us (55%)
  blocking collectives  34.3 us (20%)
  between operations  14.2 us (8%)
  starting transfers between devices  9.96 us (6%)
  matrix products  9.15 us (5%)
  local copies, waits for them, and re-layouts  5.97 us (3%)
  other arithmetic  4.17 us (2%)
    all_gather x1, waiting for transfers between devices, body(): row_piece = lax.all_gather(tokens, 'tp', axis=2, tiled=True)  82.5 us
    all_gather x1, blocking collectives, body(): new_piece = lax.all_gather(new_token, 'tp', axis=2, tiled=True)  34.3 us
    dot_general x1, matrix products, body(): jnp.dot(row_piece, row_weights, preferred_element_type=jnp.float32)  6.76 us
    all_to_all x1, starting transfers between devices, from_everyone(): return lax.all_to_all(copies, axis, split_axis=0, concat_axis=0, tiled=True)  6.41 us
    all_to_all x1, waiting for transfers between devices, from_everyone(): return lax.all_to_all(copies, axis, split_axis=0, concat_axis=0, tiled=True)  6.33 us
    all_to_all x1, waiting for transfers between devices, sent_and_summed(): lax.all_to_all(tiles, axis, split_axis=0, concat_axis=0, tiled=True)  5.1 us
    unnamed x14, local copies, waits for them, and re-layouts  4.6 us
    all_to_all x1, starting transfers between devices, sent_and_summed(): lax.all_to_all(tiles, axis, split_axis=0, concat_axis=0, tiled=True)  3.51 us
  transfers between devices with their start and end apart: 3, of which 3 were waited for; matrix products, arithmetic and copies ran while one was open for 5% of the time, Pallas kernels for 0%

commit v1 on v0

--- a/solution.py
+++ b/solution.py
@@ -55,7 +55,9 @@
     key_scale = HD ** (-0.5)
     row_weights = jnp.concatenate([key_weight, value_weight], axis=1)
     all_weights = jnp.concatenate([key_weight, value_weight, query_weight], axis=1)
-    row_piece = lax.all_gather(tokens, "tp", axis=2, tiled=True)
+    row_piece = jnp.concatenate(
+        lax.all_to_all(jnp.stack([tokens] * lax.axis_size("tp")), "tp", 0, 0), axis=2
+    )
     new_piece = lax.all_gather(new_token, "tp", axis=2, tiled=True)
     row_total = jnp.dot(row_piece, row_weights, preferred_element_type=jnp.float32)
     new_total = jnp.dot(new_piece, all_weights, preferred_element_type=jnp.float32)

time: 173 us -> 629 us (3.64)
  the two profiles are of different devices: /device:TPU:32 before, /device:TPU:2 now
where the time goes in v1:
time: 629 us; the launch traced here: 628 us
  blocking collectives  564 us (90%)
  starting transfers between devices  28 us (4%)
  local copies, waits for them, and re-layouts  13.6 us (2%)
  matrix products  9.02 us (1%)
  waiting for transfers between devices  8.85 us (1%)
    all_gather x1, blocking collectives, body(): new_piece = lax.all_gather(new_token, 'tp', axis=2, tiled=True)  564 us
    all_to_all x1, starting transfers between devices, body(): lax.all_to_all(jnp.stack([tokens] * lax.axis_size('tp')), 'tp', 0, 0)  15.7 us
  transfers between devices with their start and end apart: 3, of which 2 were waited for; matrix products, arithmetic and copies ran while one was open for 1% of the time, Pallas kernels for 0%

profile of v1, /device:TPU:2, one launch (start us, length us, event | category | flops | bytes accessed | tf_op | source)
XLA Modules:
  0.0 628.1 jit_solution(14454574913981206434)
XLA Ops:
  0.6 8.6 %stack.2 = bf16[32,3,512,128]{3,2,1,0:T(8,128)(2,1)} broadcast(bf16[3,512,128]{2,1,0:T(8,128)(2,1)} %param.6), dimensions={1,2,3} | broadcast | bytes 12976128 | tf_op jit(solution)/shard_map/stack | solution.py:59
  9.2 15.7 %all-to-all-start = ((bf16[32,3,512,128]{3,2,1,0:T(8,128)(2,1)}), bf16[32,3,512,128]{3,2,1,0:T(8,128)(2,1)}, u32[]{:S(2)}, u32[]{:S(2)}) async-start(bf16[32,3,512,128]{3,2,1,0:T(8,128)(2,1)} %stack.2), calls=%async_computation | async-start | bytes 25165824 | tf_op jit(solution)/shard_map/all_to_all | solution.py:59
  25.0 0.5 copy.28
  25.5 1.4 copy.29
  26.9 563.7 %all_gather.3 = bf16[3,1,4096]{2,0,1:T(4,128)(2,1)S(1)} all-gather(bf16[3,1,128]{2,0,1:T(4,128)(2,1)S(1)} %copy-done.3), channel_id=1, replica_groups=mesh['sp'=16,'tp'=32] {'tp'}, dimensions={2}, use_global_device_ids=true | all-gather | bytes 25344 | tf_op jit(solution)/shard_map/all_gather | solution.py:61
  590.6 1.7 fusion.11
  592.4 0.1 reshape.217
  592.8 0.3 multiply_cosine_fusion
  593.1 6.8 %fusion = f32[256,3,512]{2,0,1:T(8,128)S(1)} fusion(bf16[4096,128]{0,1:T(8,128)(2,1)} %copy.29, bf16[4096,128]{0,1:T(8,128)(2,1)S(1)} %copy.28, bf16[32,3,512,128]{3,2,1,0:T(8,128)(2,1)} %all-to-all-done), kind=kOutput, calls=%fused_computation | convolution fusion | flops 3225419776 | bytes 16252928 | tf_op jit(solution)/shard_map/dot_general | solution.py:62
  600.0 0.1 multiply_subtract_fusion
  600.2 0.3 convolution_multiply_fusion
  600.4 0.2 fusion.24
  600.8 0.7 reshape.225
  601.5 7.5 %all-to-all-start.2 = ((f32[16,1,384]{2,1,0:T(1,128)}), f32[16,1,384]{2,1,0:T(1,128)S(1)}, u32[]{:S(2)}, u32[]{:S(2)}) async-start(f32[16,1,384]{2,1,0:T(1,128)} %reshape.225), calls=%async_computation.2 | async-start | bytes 49152 | tf_op jit(solution)/shard_map/all_to_all | solution.py:23
  608.9 0.2 multiply_reduce_fusion.1
  609.2 0.1 mul.280
  609.3 0.1 reshape.218
  609.4 0.8 reshape.223
  610.2 5.0 all-to-all-done.2
  615.2 4.8 all-to-all-start.1
  619.9 0.5 broadcast.166
  620.4 0.7 reduce.1
  621.2 0.1 reshape.226
  621.3 0.2 fusion.34
  621.5 0.2 multiply_reduce_fusion
  621.8 0.1 mul.285
  621.9 0.1 sub.42
  622.0 0.6 multiply_convert_fusion.2
  622.6 3.9 all-to-all-done.1
  626.5 0.9 reduce
  627.4 0.1 reshape.224
  627.5 0.7 reduce_sum.47
  (30 shorter events, 0.9 us)
Async XLA Ops:
  9.2 15.8 %copy-start.1 = (bf16[4096,128]{1,0:T(8,128)(2,1)S(1)}, bf16[4096,128]{1,0:T(8,128)(2,1)}, u32[]{:S(2)}) copy-start(bf16[4096,128]{1,0:T(8,128)(2,1)} %param.9) | copy-start | bytes 3145732
  9.2 16.3 %copy-start = (bf16[4096,128]{1,0:T(8,128)(2,1)S(1)}, bf16[4096,128]{1,0:T(8,128)(2,1)}, u32[]{:S(2)}) copy-start(bf16[4096,128]{1,0:T(8,128)(2,1)} %param.10) | copy-start | bytes 3145732
  9.2 583.9 %all-to-all-start = ((bf16[32,3,512,128]{3,2,1,0:T(8,128)(2,1)}), bf16[32,3,512,128]{3,2,1,0:T(8,128)(2,1)}, u32[]{:S(2)}, u32[]{:S(2)}) async-start(bf16[32,3,512,128]{3,2,1,0:T(8,128)(2,1)} %stack.2), calls=%async_computation | async-start | bytes 25165824 | tf_op jit(solution)/shard_map/all_to_all | solution.py:59
  25.0 1.9 copy-start.3
  590.6 2.1 copy-start.2
  601.5 13.7 %all-to-all-start.2 = ((f32[16,1,384]{2,1,0:T(1,128)}), f32[16,1,384]{2,1,0:T(1,128)S(1)}, u32[]{:S(2)}, u32[]{:S(2)}) async-start(f32[16,1,384]{2,1,0:T(1,128)} %reshape.225), calls=%async_computation.2 | async-start | bytes 49152 | tf_op jit(solution)/shard_map/all_to_all | solution.py:23
  615.2 11.3 %all-to-all-start.1 = ((f32[16,1,1536]{2,1,0:T(1,128)}), f32[16,1,1536]{2,1,0:T(1,128)S(1)}, u32[]{:S(2)}, u32[]{:S(2)}) async-start(f32[16,1,1536]{2,1,0:T(1,128)} %reshape.223), calls=%async_computation.1 | async-start | bytes 196608 | tf_op jit(solution)/shard_map/all_to_all | solution.py:17
